TPU v7x, 32 devices: a whole 2x2x4 slice. The times are simulated.
32 devices in a mesh: grp: 2 (over y), ra: 4 (over z), cb: 4 (over x, core).
Axes of the slice: x: 2, y: 2, z: 4, core: 2. Of those that a mesh axis runs over, the one named last changes fastest.
Arguments:
- tokens: bfloat16 [512, 4096], P('grp', 'ra'), parts along dimension 0, may hold values from -30 to 30, as said below
- norm_gain: bfloat16 [4096], P('ra'), may hold values from 0.099609375 to 1.8984375
- w_gate: bfloat16 [4096, 11264], P('ra', 'cb'), may hold values from -0.09375 to 0.09375
- w_value: bfloat16 [4096, 11264], P('ra', 'cb'), may hold values from -0.09375 to 0.09375
- conv_gate: float32 [3, 11264], P(None, 'cb'), may hold values from -3 to 3
- conv_value: float32 [3, 11264], P(None, 'cb'), may hold values from -3 to 3
- bias_gate: float32 [11264], P('cb'), may hold values from -3 to 3
- bias_value: float32 [11264], P('cb'), may hold values from -3 to 3
- w_down: bfloat16 [11264, 4096], P('cb', 'ra'), may hold values from -1 to 1
- out_gain: bfloat16 [4096], P('ra'), may hold values from 0.099609375 to 1.8984375
Outputs:
- normed_out: bfloat16 [512, 4096], P('grp', 'ra'), parts along dimension 0
There are 2 independent parts, one for each index of `grp`. A program takes and returns all parts, laid end to end along the dimension named above; an argument that names none is the same for every part. Nothing has to cross between parts.
Inputs may be any that keep to these rules, and one draw needn't show every extreme that they name: `tokens`: feature scales differ along the width.
All inputs are finite; a program needn't handle non-finite values.
Results may differ from a plain program's by a relative error of at most 0.0059.
Values may be sent and summed in bfloat16 or wider, within the bound.
A program may use at most 64 MiB of HBM per device.

v0:
```python
import jax
import jax.numpy as jnp
from jax import lax
from jax.sharding import PartitionSpec as P

EPSILON = 1e-06
RESIDUAL_WEIGHT = 0.25


def spread(signal, kernel):
    padded = jnp.pad(signal, ((1, 1), (0, 0)))
    return padded[:-2] * kernel[0] + padded[1:-1] * kernel[1] + padded[2:] * kernel[2]


def activate(gate_sum, value_sum, kernel_gate, kernel_value, offset_gate, offset_value):
    gate_conv = spread(gate_sum, kernel_gate) + offset_gate
    value_conv = spread(value_sum, kernel_value) + offset_value
    return (jax.nn.silu(gate_conv) * value_conv).astype(jnp.bfloat16)


def body(
    tokens,
    norm_gain,
    w_gate,
    w_value,
    conv_gate,
    conv_value,
    bias_gate,
    bias_value,
    w_down,
    out_gain,
):
    wide_in = tokens.astype(jnp.float32)
    width = wide_in.shape[1] * lax.axis_size("ra")
    squares = lax.psum(jnp.sum(wide_in * wide_in, axis=1), "ra")
    rscale = lax.rsqrt(squares / width + EPSILON)
    normed = (wide_in * rscale[:, None] * norm_gain.astype(jnp.float32)).astype(jnp.bfloat16)
    part_gate = jnp.dot(normed, w_gate, preferred_element_type=jnp.float32)
    part_value = jnp.dot(normed, w_value, preferred_element_type=jnp.float32)
    gate_sum, value_sum = (
        lax.psum_scatter(part_gate, "ra", scatter_dimension=1, tiled=True),
        lax.psum_scatter(part_value, "ra", scatter_dimension=1, tiled=True),
    )
    share_cols = gate_sum.shape[1]
    first_col = lax.axis_index("ra") * share_cols
    local_hidden = activate(
        gate_sum,
        value_sum,
        lax.dynamic_slice_in_dim(conv_gate, first_col, share_cols, 1),
        lax.dynamic_slice_in_dim(conv_value, first_col, share_cols, 1),
        lax.dynamic_slice_in_dim(bias_gate, first_col, share_cols, 0),
        lax.dynamic_slice_in_dim(bias_value, first_col, share_cols, 0),
    )
    partial_value = jnp.dot(
        lax.all_gather(local_hidden, "ra", axis=1, tiled=True),
        w_down,
        preferred_element_type=jnp.float32,
    )
    branch = lax.psum(partial_value, "cb")
    summed = RESIDUAL_WEIGHT * wide_in + branch
    totals = lax.psum(jnp.sum(summed * summed, axis=1), "ra")
    oscale = lax.rsqrt(totals / width + EPSILON)
    return (summed * oscale[:, None] * out_gain.astype(jnp.float32)).astype(jnp.bfloat16)


def solution(mesh):
    return jax.shard_map(
        body,
        mesh=mesh,
        in_specs=(
            P("grp", "ra"),
            P("ra"),
            P("ra", "cb"),
            P("ra", "cb"),
            P(None, "cb"),
            P(None, "cb"),
            P("cb"),
            P("cb"),
            P("cb", "ra"),
            P("ra"),
        ),
        out_specs=P("grp", "ra"),
        check_vma=False,
    )
```

profile of v0, /device:TPU:0, one launch (start us, length us, event | category | flops | bytes accessed | tf_op | source)
XLA Modules:
  0.0 244.4 jit_solution(13220206293900376885)
XLA Ops:
  6.5 0.0 reduce-scatter.5.cloned.1.call-start
  6.5 0.7 convert_element_type.22
  7.2 1.2 fusion.1
  8.4 13.5 %psum.21 = f32[256]{0:T(256)S(1)} all-reduce(f32[256]{0:T(256)S(1)} %fusion.1), channel_id=1, replica_groups=mesh['grp'=2,'ra'=4,'cb'=4] {'ra'}, use_global_device_ids=true, to_apply=%region_1.0 | all-reduce | flops 256 | bytes 2048 | tf_op jit(solution)/shard_map/psum | solution.py:35
  21.9 0.0 copy-start
  21.9 6.9 %fusion.16 = f32[256,2816]{0,1:T(8,128)} fusion(bf16[1024,2816]{1,0:T(8,128)(2,1)} %param.13, bf16[256,1024]{1,0:T(8,128)(2,1)} %param.10, f32[1024]{0:T(1024)S(1)} %convert_element_type.22, f32[256]{0:T(256)S(1)} %add_rsqrt_fusion.1), kind=kOutput, calls=%fused_computation.25 | convolution fusion | flops 1477443584 | bytes 9180160 | tf_op jit(solution)/shard_map/dot_general | solution.py:39
  28.8 0.0 reduce-scatter.5.cloned.1.call-update
  28.8 0.0 reduce-scatter.3.cloned.1.call-start
  28.9 0.0 copy-done
  28.9 6.7 %fusion.18 = f32[256,2816]{0,1:T(8,128)} fusion(bf16[1024,2816]{1,0:T(8,128)(2,1)} %param.12, bf16[256,1024]{1,0:T(8,128)(2,1)S(1)} %copy-done, f32[1024]{0:T(1024)S(1)} %convert_element_type.22, f32[256]{0:T(256)S(1)} %add_rsqrt_fusion.1), kind=kOutput, calls=%fused_computation.26 | convolution fusion | flops 1477443584 | bytes 9180160 | tf_op jit(solution)/shard_map/dot_general | solution.py:38
  35.5 0.0 reduce-scatter.3.cloned.1.call-update
  35.6 0.0 all-gather.2.cloned.1.call-start
  35.6 0.8 dynamic_slice.15
  36.4 0.8 dynamic_slice.13
  37.2 0.9 dynamic-slice_reduce_fusion.2
  38.1 45.4 %reduce-scatter.5.cloned.1.call-done = f32[256,704]{0,1:T(8,128)} async-done(((f32[256,2816]{0,1:T(8,128)}), f32[256,704]{0,1:T(8,128)}) %reduce-scatter.5.cloned.1.call-update) | async-done | bytes 720912 | tf_op jit(solution)/shard_map/reduce_scatter | solution.py:42
  83.5 58.4 %reduce-scatter.3.cloned.1.call-done = f32[256,704]{0,1:T(8,128)} async-done(((f32[256,2816]{0,1:T(8,128)}), f32[256,704]{0,1:T(8,128)}) %reduce-scatter.3.cloned.1.call-update) | async-done | bytes 720912 | tf_op jit(solution)/shard_map/reduce_scatter | solution.py:41
  141.9 4.6 %fusion.14 = bf16[256,704]{0,1:T(8,128)(2,1)} fusion(f32[256,704]{0,1:T(8,128)} %reduce-scatter.5.cloned.1.call-done, f32[256,704]{0,1:T(8,128)} %reduce-scatter.3.cloned.1.call-done, f32[704]{0:T(1024)S(1)} %dynamic_slice.15, f32[704]{0:T(1024)S(1)} %get-tuple-element.10, f32[704]{0:T(1024)S(1)} %get-tuple-element.9, f32[704]{0:T(1024)S(1)} %get-tuple-element.8, ...), kind=kLoop, calls=%fused_computation.23 | loop fusion | flops 3244032 | bytes 1824768 | tf_op jit(solution)/shard_map/convert_element_type | solution.py:18
  146.6 0.0 all-gather.2.cloned.1.call-update
  146.6 0.0 copy-start.1
  146.6 0.0 all-reduce.4.cloned.1.call-start
  146.6 34.6 %all-gather.2.cloned.1.call-done = bf16[256,2816]{0,1:T(8,128)(2,1)} async-done(((bf16[256,704]{0,1:T(8,128)(2,1)}), bf16[256,2816]{0,1:T(8,128)(2,1)}) %all-gather.2.cloned.1.call-update) | async-done | bytes 1441808 | tf_op jit(solution)/shard_map/all_gather | solution.py:55
  181.2 5.7 %fusion.20 = f32[256,1024]{1,0:T(8,128)} fusion(bf16[256,2816]{0,1:T(8,128)(2,1)} %all-gather.2.cloned.1.call-done, bf16[2816,1024]{1,0:T(8,128)(2,1)} %param.18), kind=kOutput, calls=%fused_computation.35 | convolution fusion | flops 1476395008 | bytes 8257536 | tf_op jit(solution)/shard_map/dot_general | solution.py:54
  187.0 0.0 all-reduce.4.cloned.1.call-update
  187.0 0.0 copy-done.1
  187.0 35.4 %all-reduce.4.cloned.1.call-done = f32[256,1024]{1,0:T(8,128)} async-done(((f32[256,1024]{1,0:T(8,128)}), f32[256,1024]{1,0:T(8,128)}) %all-reduce.4.cloned.1.call-update) | async-done | bytes 1048592 | tf_op jit(solution)/shard_map/psum | solution.py:59
  222.4 1.5 multiply_reduce_fusion
  223.9 11.7 %psum.23 = f32[256]{0:T(256)S(1)} all-reduce(f32[256]{0:T(256)S(1)} %multiply_reduce_fusion), channel_id=1, replica_groups=mesh['grp'=2,'ra'=4,'cb'=4] {'ra'}, use_global_device_ids=true, to_apply=%region_6.7 | all-reduce | flops 256 | bytes 2048 | tf_op jit(solution)/shard_map/psum | solution.py:61
  235.6 2.2 multiply_convert_fusion
  (3 shorter events, 0.0 us)
Async XLA Ops:
  6.5 77.0 %reduce-scatter.5.cloned.1.call-start = ((), (), s32[]{:S(2)}) async-start(), calls=%async_computation.3 | async-start | bytes 3604480 | tf_op jit(solution)/shard_map/reduce_scatter | solution.py:42
  21.9 6.9 %copy-start = (bf16[256,1024]{1,0:T(8,128)(2,1)S(1)}, bf16[256,1024]{1,0:T(8,128)(2,1)}, u32[]{:S(2)}) copy-start(bf16[256,1024]{1,0:T(8,128)(2,1)} %param.10) | copy-start | bytes 1572868
  28.8 113.1 %reduce-scatter.3.cloned.1.call-start = ((), (), s32[]{:S(2)}) async-start(), calls=%async_computation.2 | async-start | bytes 3604480 | tf_op jit(solution)/shard_map/reduce_scatter | solution.py:41
  35.6 145.7 %all-gather.2.cloned.1.call-start = ((), (), s32[]{:S(2)}) async-start(), calls=%async_computation.4 | async-start | bytes 1802240 | tf_op jit(solution)/shard_map/all_gather | solution.py:55
  146.6 40.4 %copy-start.1 = (bf16[1024]{0:T(1024)(128)(2,1)S(1)}, bf16[1024]{0:T(1024)(128)(2,1)}, u32[]{:S(2)}) copy-start(bf16[1024]{0:T(1024)(128)(2,1)} %param.19) | copy-start | bytes 6148
  146.6 75.8 %all-reduce.4.cloned.1.call-start = ((), (), s32[]{:S(2)}) async-start(), calls=%async_computation.5 | async-start | bytes 2097152 | tf_op jit(solution)/shard_map/psum | solution.py:59
Sparse Core Ops, SparseCore 0:
  28.9 54.5 reduce-scatter.4
  85.8 56.0 reduce-scatter.2
  146.7 34.4 all-gather.1
  187.1 35.2 all-reduce.3
where the time goes:
time: 245 us; the launch traced here: 244 us
  waiting for transfers between devices  174 us (71%)
  blocking collectives  25.2 us (10%)
  matrix products  19.3 us (8%)
  between operations  13.2 us (5%)
  other arithmetic  10.3 us (4%)
  local copies, waits for them, and re-layouts  2.5 us (1%)
    reduce_scatter x1, waiting for transfers between devices, body(): lax.psum_scatter(part_gate, 'ra', scatter_dimension=1, tiled=True)  58.4 us
    reduce_scatter x1, waiting for transfers between devices, body(): lax.psum_scatter(part_value, 'ra', scatter_dimension=1, tiled=True)  45.4 us
    psum x1, waiting for transfers between devices, body(): branch = lax.psum(partial_value, 'cb')  35.4 us
    all_gather x1, waiting for transfers between devices, body(): lax.all_gather(local_hidden, 'ra', axis=1, tiled=True)  34.6 us
    psum x1, blocking collectives, body(): squares = lax.psum(jnp.sum(wide_in * wide_in, axis=1), 'ra')  13.5 us
    psum x1, blocking collectives, body(): totals = lax.psum(jnp.sum(summed * summed, axis=1), 'ra')  11.7 us
    dot_general x1, matrix products, body(): part_value = jnp.dot(normed, w_value, preferred_element_type=jnp.float32)  6.85 us
    dot_general x1, matrix products, body(): part_gate = jnp.dot(normed, w_gate, preferred_element_type=jnp.float32)  6.67 us
  transfers between devices with their start and end apart: 4, of which 4 were waited for; matrix products, arithmetic and copies ran while one was open for 4% of the time, Pallas kernels for 0%

commit v1 on v0

--- a/solution.py
+++ b/solution.py
@@ -52,7 +52,7 @@
         lax.dynamic_slice_in_dim(bias_value, first_col, share_cols, 0),
     )
     partial_value = jnp.dot(
-        lax.all_gather(local_hidden, "ra", axis=1, tiled=True),
+        jnp.concatenate(lax.all_gather(local_hidden, "ra"), axis=1),
         w_down,
         preferred_element_type=jnp.float32,
     )

time: 245 us -> 246 us (level)
  no operation moved by 1% of the time
where the time goes in v1:
time: 246 us; the launch traced here: 245 us
  waiting for transfers between devices  174 us (71%)
  blocking collectives  25.2 us (10%)
  matrix products  18.9 us (8%)
  between operations  13.2 us (5%)
  other arithmetic  10.3 us (4%)
  local copies, waits for them, and re-layouts  3.95 us (2%)
    reduce_scatter x1, waiting for transfers between devices, body(): lax.psum_scatter(part_gate, 'ra', scatter_dimension=1, tiled=True)  58.4 us
    reduce_scatter x1, waiting for transfers between devices, body(): lax.psum_scatter(part_value, 'ra', scatter_dimension=1, tiled=True)  45.4 us
    all_gather x1, waiting for transfers between devices, body(): lax.all_gather(local_hidden, 'ra')  35.4 us
    psum x1, waiting for transfers between devices, body(): branch = lax.psum(partial_value, 'cb')  34.6 us
    psum x1, blocking collectives, body(): squares = lax.psum(jnp.sum(wide_in * wide_in, axis=1), 'ra')  13.5 us
    psum x1, blocking collectives, body(): totals = lax.psum(jnp.sum(summed * summed, axis=1), 'ra')  11.7 us
    dot_general x1, matrix products, body(): part_value = jnp.dot(normed, w_value, preferred_element_type=jnp.float32)  6.85 us
    dot_general x1, matrix products, body(): part_gate = jnp.dot(normed, w_gate, preferred_element_type=jnp.float32)  6.67 us
  transfers between devices with their start and end apart: 4, of which 4 were waited for; matrix products, arithmetic and copies ran while one was open for 4% of the time, Pallas kernels for 0%

profile of v1, /device:TPU:0, one launch (start us, length us, event | category | flops | bytes accessed | tf_op | source)
XLA Modules:
  0.0 245.5 jit_solution(17280826574055454875)
XLA Ops:
  6.5 0.0 reduce-scatter.5.cloned.1.call-start
  6.5 0.7 convert_element_type.22
  7.2 1.2 fusion.1
  8.4 13.5 %psum.21 = f32[256]{0:T(256)S(1)} all-reduce(f32[256]{0:T(256)S(1)} %fusion.1), channel_id=1, replica_groups=mesh['grp'=2,'ra'=4,'cb'=4] {'ra'}, use_global_device_ids=true, to_apply=%region_1.0 | all-reduce | flops 256 | bytes 2048 | tf_op jit(solution)/shard_map/psum | solution.py:35
  21.9 0.0 copy-start
  21.9 6.9 %fusion.16 = f32[256,2816]{0,1:T(8,128)} fusion(bf16[1024,2816]{1,0:T(8,128)(2,1)} %param.13, bf16[256,1024]{1,0:T(8,128)(2,1)} %param.10, f32[1024]{0:T(1024)S(1)} %convert_element_type.22, f32[256]{0:T(256)S(1)} %add_rsqrt_fusion.1), kind=kOutput, calls=%fused_computation.26 | convolution fusion | flops 1477443584 | bytes 9180160 | tf_op jit(solution)/shard_map/dot_general | solution.py:39
  28.8 0.0 reduce-scatter.5.cloned.1.call-update
  28.8 0.0 reduce-scatter.3.cloned.1.call-start
  28.9 0.0 copy-done
  28.9 6.7 %fusion.18 = f32[256,2816]{0,1:T(8,128)} fusion(bf16[1024,2816]{1,0:T(8,128)(2,1)} %param.12, bf16[256,1024]{1,0:T(8,128)(2,1)S(1)} %copy-done, f32[1024]{0:T(1024)S(1)} %convert_element_type.22, f32[256]{0:T(256)S(1)} %add_rsqrt_fusion.1), kind=kOutput, calls=%fused_computation.27 | convolution fusion | flops 1477443584 | bytes 9180160 | tf_op jit(solution)/shard_map/dot_general | solution.py:38
  35.5 0.0 reduce-scatter.3.cloned.1.call-update
  35.6 0.0 all-gather.3.cloned.1.call-start
  35.6 0.8 dynamic_slice.15
  36.4 0.8 dynamic_slice.13
  37.2 0.9 dynamic-slice_reduce_fusion.2
  38.1 45.4 %reduce-scatter.5.cloned.1.call-done = f32[256,704]{0,1:T(8,128)} async-done(((f32[256,2816]{0,1:T(8,128)}), f32[256,704]{0,1:T(8,128)}) %reduce-scatter.5.cloned.1.call-update) | async-done | bytes 720912 | tf_op jit(solution)/shard_map/reduce_scatter | solution.py:42
  83.5 58.4 %reduce-scatter.3.cloned.1.call-done = f32[256,704]{0,1:T(8,128)} async-done(((f32[256,2816]{0,1:T(8,128)}), f32[256,704]{0,1:T(8,128)}) %reduce-scatter.3.cloned.1.call-update) | async-done | bytes 720912 | tf_op jit(solution)/shard_map/reduce_scatter | solution.py:41
  141.9 4.6 %fusion.14 = bf16[256,704]{0,1:T(8,128)(2,1)} fusion(f32[256,704]{0,1:T(8,128)} %reduce-scatter.5.cloned.1.call-done, f32[256,704]{0,1:T(8,128)} %reduce-scatter.3.cloned.1.call-done, f32[704]{0:T(1024)S(1)} %dynamic_slice.15, f32[704]{0:T(1024)S(1)} %get-tuple-element.10, f32[704]{0:T(1024)S(1)} %get-tuple-element.9, f32[704]{0:T(1024)S(1)} %get-tuple-element.8, ...), kind=kLoop, calls=%fused_computation.24 | loop fusion | flops 3244032 | bytes 1824768 | tf_op jit(solution)/shard_map/convert_element_type | solution.py:18
  146.6 0.0 all-gather.3.cloned.1.call-update
  146.6 0.0 all-reduce.4.cloned.1.call-start
  146.6 35.4 %all-gather.3.cloned.1.call-done = bf16[1024,704]{0,1:T(8,128)(2,1)} async-done(((bf16[256,704]{0,1:T(8,128)(2,1)}), bf16[1024,704]{0,1:T(8,128)(2,1)}) %all-gather.3.cloned.1.call-update) | async-done | bytes 1441808 | tf_op jit(solution)/shard_map/all_gather | solution.py:55
  182.1 1.5 copy.14
  183.5 0.0 copy-start.1
  183.5 5.4 %fusion.20 = f32[256,1024]{1,0:T(8,128)} fusion(bf16[256,2816]{0,1:T(8,128)(2,1)S(1)} %bitcast.11, bf16[2816,1024]{1,0:T(8,128)(2,1)} %param.18), kind=kOutput, calls=%fused_computation.36 | convolution fusion | flops 1476395008 | bytes 8257536 | tf_op jit(solution)/shard_map/dot_general | solution.py:54
  188.9 0.0 all-reduce.4.cloned.1.call-update
  188.9 0.0 copy-done.1
  188.9 34.6 %all-reduce.4.cloned.1.call-done = f32[256,1024]{1,0:T(8,128)} async-done(((f32[256,1024]{1,0:T(8,128)}), f32[256,1024]{1,0:T(8,128)}) %all-reduce.4.cloned.1.call-update) | async-done | bytes 1048592 | tf_op jit(solution)/shard_map/psum | solution.py:59
  223.6 1.5 multiply_reduce_fusion
  225.0 11.7 %psum.23 = f32[256]{0:T(256)S(1)} all-reduce(f32[256]{0:T(256)S(1)} %multiply_reduce_fusion), channel_id=1, replica_groups=mesh['grp'=2,'ra'=4,'cb'=4] {'ra'}, use_global_device_ids=true, to_apply=%region_6.7 | all-reduce | flops 256 | bytes 2048 | tf_op jit(solution)/shard_map/psum | solution.py:61
  236.7 2.2 multiply_convert_fusion
  (3 shorter events, 0.0 us)
Async XLA Ops:
  6.5 77.0 %reduce-scatter.5.cloned.1.call-start = ((), (), s32[]{:S(2)}) async-start(), calls=%async_computation.3 | async-start | bytes 3604480 | tf_op jit(solution)/shard_map/reduce_scatter | solution.py:42
  21.9 6.9 %copy-start = (bf16[256,1024]{1,0:T(8,128)(2,1)S(1)}, bf16[256,1024]{1,0:T(8,128)(2,1)}, u32[]{:S(2)}) copy-start(bf16[256,1024]{1,0:T(8,128)(2,1)} %param.10) | copy-start | bytes 1572868
  28.8 113.1 %reduce-scatter.3.cloned.1.call-start = ((), (), s32[]{:S(2)}) async-start(), calls=%async_computation.2 | async-start | bytes 3604480 | tf_op jit(solution)/shard_map/reduce_scatter | solution.py:41
  35.6 146.5 %all-gather.3.cloned.1.call-start = ((), (), s32[]{:S(2)}) async-start(), calls=%async_computation.5 | async-start | bytes 1802240 | tf_op jit(solution)/shard_map/all_gather | solution.py:55
  146.6 77.0 %all-reduce.4.cloned.1.call-start = ((), (), s32[]{:S(2)}) async-start(), calls=%async_computation.4 | async-start | bytes 2097152 | tf_op jit(solution)/shard_map/psum | solution.py:59
  183.5 5.4 %copy-start.1 = (bf16[1024]{0:T(1024)(128)(2,1)S(1)}, bf16[1024]{0:T(1024)(128)(2,1)}, u32[]{:S(2)}) copy-start(bf16[1024]{0:T(1024)(128)(2,1)} %param.19) | copy-start | bytes 6148
Sparse Core Ops, SparseCore 0:
  28.9 54.5 reduce-scatter.4
  85.8 56.0 reduce-scatter.2
  146.7 35.3 all-gather.2
  189.0 34.4 all-reduce.3
